TPU v7x, 256 devices: a whole 4x4x8 slice. The times are simulated.
256 devices in a mesh: ep: 64 (over z, y, core), tp: 4 (over x).
Axes of the slice: x: 4, y: 4, z: 8, core: 2. Of those that a mesh axis runs over, the one named last changes fastest.
Arguments:
- tokens: bfloat16 [49152, 2048], P('ep', 'tp')
- norm_gain: float32 [2048], P('tp'), may hold values from 0.1 to 1.9
- routing: int32 [49152, 2], P('ep'), may hold values from 0 to 63, as said below
- route_weight: float32 [49152, 2], P('ep'), may hold values from 0.2 to 1
- w_gate: bfloat16 [64, 2048, 512], P('ep', 'tp'), may hold values from -0.125 to 0.125
- w_up: bfloat16 [64, 2048, 512], P('ep', 'tp'), may hold values from -0.125 to 0.125
- w_down: bfloat16 [64, 512, 2048], P('ep', None, 'tp'), may hold values from -0.25 to 0.25
- w_branch_in: bfloat16 [2048, 1024], P('ep', 'tp'), may hold values from -0.125 to 0.125
- w_branch_out: bfloat16 [1024, 2048], P('tp', 'ep'), may hold values from -0.1875 to 0.1875
- branch_gate: float32 [2048], P('tp'), may hold values from -3 to 3
Outputs:
- mixed: bfloat16 [49152, 2048], P('ep', 'tp')
Inputs may be any that keep to these rules, and one draw needn't show every extreme that they name: `routing`: each row names two different experts of the same group; expert e belongs to group e // 16. Among the rows of one device (aligned blocks of 768 rows) no expert is named more than 48 times, and in every block all experts of one group are named exactly 48 times.
All inputs are finite; a program needn't handle non-finite values.
Results may differ from a plain program's by a relative error of at most 0.0069.
Values may be sent and summed in bfloat16 or wider, within the bound.
A program may use at most 128 MiB of HBM per device.

v0:
```python
import jax
import jax.numpy as jnp
from jax import lax
from jax.sharding import PartitionSpec as P

GROUPS = 4
epsilon = 1e-06


def sent_to_all(value, axis):
    size = lax.axis_size(axis)
    return lax.all_to_all(
        jnp.broadcast_to(value[None], (size, *value.shape)), axis, 0, 0, tiled=True
    )


def taken_together(value, axis):
    return sent_to_all(value, axis).sum(axis=0)


def gather_turned(arrays, axis, dims):
    turned = [jnp.moveaxis(a, dim, 0) for a, dim in zip(arrays, dims)]
    both = jnp.concatenate([t.reshape(len(t), -1) for t in turned], axis=1)
    filled, at, gathered = (lax.all_gather(both, axis, axis=0, tiled=True), 0, [])
    for t, dim in zip(turned, dims):
        share = filled[:, at : at + t[0].size].reshape(-1, *t.shape[1:])
        gathered.append(jnp.moveaxis(share, 0, dim))
        at += t[0].size
    return tuple(gathered)


def send_back(result):
    return lax.all_to_all(result, "ep", split_axis=0, concat_axis=0, tiled=True)


def body(
    tokens,
    norm_gain,
    routing,
    route_weight,
    w_gate,
    w_up,
    w_down,
    w_branch_in,
    w_branch_out,
    branch_gate,
):
    token_count, quarter = tokens.shape
    full_width = quarter * lax.axis_size("tp")
    floats = tokens.astype(jnp.float32)
    squares = taken_together(jnp.sum(floats * floats, axis=1), "tp")
    normed = (floats * lax.rsqrt(squares[:, None] / full_width + epsilon) * norm_gain).astype(
        jnp.bfloat16
    )
    expert_count = lax.axis_size("ep") * w_gate.shape[0]
    capacity = token_count // (expert_count // GROUPS)
    flat_ids = routing.reshape(-1)
    one_hot = (flat_ids[:, None] == jnp.arange(expert_count, dtype=jnp.int32)[None, :]).astype(
        jnp.int32
    )
    before = jnp.cumsum(one_hot, axis=0) - one_hot
    position = flat_ids * capacity + jnp.sum(before * one_hot, axis=1)
    copies = jnp.repeat(normed, 2, axis=0)
    buffer = jnp.zeros((expert_count * capacity, quarter), jnp.bfloat16).at[position].set(copies)
    buffer = buffer.reshape(expert_count, capacity, quarter)
    gate_whole, up_whole, down_whole = (
        lax.all_gather(w_gate[0], "tp", axis=0, tiled=True),
        lax.all_gather(w_up[0], "tp", axis=0, tiled=True),
        lax.all_gather(w_down[0], "tp", axis=1, tiled=True),
    )
    row_split = lax.all_to_all(
        lax.all_to_all(buffer, "ep", split_axis=0, concat_axis=0, tiled=True),
        "tp",
        split_axis=0,
        concat_axis=2,
        tiled=True,
    )
    slot_rows = row_split.reshape(-1, row_split.shape[2])
    gate_sum = jnp.dot(slot_rows, gate_whole, preferred_element_type=jnp.float32)
    up_sum = jnp.dot(slot_rows, up_whole, preferred_element_type=jnp.float32)
    hidden = (jax.nn.silu(gate_sum) * up_sum).astype(jnp.bfloat16)
    result = jnp.dot(hidden, down_whole, preferred_element_type=jnp.float32).astype(jnp.bfloat16)
    feature_split = lax.all_to_all(
        result.reshape(row_split.shape), "tp", split_axis=2, concat_axis=0, tiled=True
    )
    returned = send_back(feature_split)
    picked = returned.reshape(expert_count * capacity, quarter)[position].reshape(
        token_count, 2, quarter
    )
    routed = jnp.sum(picked.astype(jnp.float32) * route_weight[:, :, None], axis=1)
    branch_tokens = lax.all_to_all(normed, "tp", split_axis=0, concat_axis=1, tiled=True)
    in_cols, out_rows = gather_turned((w_branch_in, w_branch_out), "tp", (1, 0))
    in_whole, out_whole = gather_turned((in_cols, out_rows), "ep", (0, 1))
    branch_hidden = jax.nn.silu(
        jnp.dot(branch_tokens, in_whole, preferred_element_type=jnp.float32)
    ).astype(jnp.bfloat16)
    branch_local = jnp.dot(branch_hidden, out_whole, preferred_element_type=jnp.float32).astype(
        jnp.bfloat16
    )
    branch = lax.all_to_all(branch_local, "tp", split_axis=1, concat_axis=0, tiled=True)
    return (routed + jax.nn.sigmoid(branch_gate) * branch.astype(jnp.float32)).astype(jnp.bfloat16)


def solution(mesh):
    return jax.shard_map(
        body,
        mesh=mesh,
        in_specs=(
            P("ep", "tp"),
            P("tp"),
            P("ep", None),
            P("ep", None),
            P("ep", "tp", None),
            P("ep", "tp", None),
            P("ep", None, "tp"),
            P("ep", "tp"),
            P("tp", "ep"),
            P("tp"),
        ),
        out_specs=P("ep", "tp"),
        check_vma=False,
    )
```

profile of v0, /device:TPU:2, one launch (start us, length us, event | category | flops | bytes accessed | tf_op | source)
XLA Modules:
  0.0 391.7 jit_solution(14819414351238019944)
XLA Ops:
  6.5 0.0 all-gather.10.cloned.1.call-start
  6.5 0.7 all-gather.10.cloned.1.call-update
  7.3 0.0 all-gather.12.cloned.1.call-start
  7.3 0.7 all-gather.12.cloned.1.call-update
  8.0 1.4 fusion.12
  9.4 0.6 broadcast_in_dim.7
  10.0 5.5 %all-to-all-start = ((f32[4,1,768]{2,1,0:T(1,128)}), f32[4,1,768]{2,1,0:T(1,128)S(1)}, u32[]{:S(2)}, u32[]{:S(2)}) async-start(f32[4,1,768]{2,1,0:T(1,128)} %broadcast_in_dim.7), calls=%async_computation | async-start | bytes 24576 | tf_op jit(solution)/shard_map/all_to_all | solution.py:12
  15.4 0.0 all-gather.14.cloned.1.call-start
  15.4 0.7 all-gather.14.cloned.1.call-update
  16.2 0.0 copy-done.2
  16.2 0.2 copy.56
  16.4 0.2 eq.29
  16.6 0.2 eq.25
  16.9 18.1 %reduce-window.6 = s32[64,12,128]{2,1,0:T(8,128)S(1)} reduce-window(s32[64,12,128]{2,1,0:T(8,128)S(1)} %fusion.27, s32[]{:T(128)} %constant.6.clone.1), window={size=1x1x128 pad=0_0x0_0x127_0}, to_apply=%region_0.0 | reduce-window | flops 12484608 | bytes 786436 | tf_op jit(solution)/shard_map/reduce-window
  35.0 0.2 slice.26
  35.2 0.3 copy.58
  35.5 0.1 copy.59
  35.6 0.2 copy.55
  35.8 0.3 mul.67
  36.1 0.2 broadcast_add_fusion
  36.3 0.2 fusion.30
  36.5 0.0 all-to-all-done
  36.5 0.0 copy-done.1
  36.6 0.0 copy-done.7
  36.6 0.2 fusion.14
  36.8 0.0 copy-start
  36.8 0.9 copy-done
  37.7 0.8 broadcast_in_dim.8
  38.5 0.6 reshape.110
  39.2 9.5 %scatter_custom_fusion = bf16[3072,512]{1,0:T(8,128)(2,1)} fusion(s32[1536]{0:T(1024)S(1)} %fusion.32, bf16[1536,512]{1,0:T(8,128)(2,1)S(1)} %reshape.110, bf16[]{:T(256)} %constant.8.clone.1), kind=kCustom, calls=%fused_computation.23 | custom fusion | bytes 3145730 | tf_op jit(solution)/shard_map/scatter | solution.py:64
  48.7 11.6 %all-to-all-start.1 = ((bf16[64,48,512]{2,1,0:T(8,128)(2,1)}), bf16[64,48,512]{2,1,0:T(8,128)(2,1)S(1)}, u32[]{:S(2)}, u32[]{:S(2)}) async-start(bf16[64,48,512]{2,1,0:T(8,128)(2,1)} %bitcast.74), calls=%async_computation.1 | async-start | bytes 6291456 | tf_op jit(solution)/shard_map/all_to_all | solution.py:72
  60.3 0.0 all-gather.8.cloned.1.call-start
  60.3 0.0 copy-done.3
  60.4 12.7 %all_gather.18 = bf16[1024,64]{0,1:T(8,128)(2,1)S(1)} all-gather(bf16[256,64]{0,1:T(8,128)(2,1)S(1)} %pad_maximum_fusion.1), channel_id=1, replica_groups=mesh['ep'=64,'tp'=4] {'tp'}, dimensions={0}, use_global_device_ids=true | all-gather | bytes 163840 | tf_op jit(solution)/shard_map/all_gather | solution.py:24
  73.1 0.7 pad_maximum_fusion
  73.7 0.0 all-gather.8.cloned.1.call-update
  73.7 60.4 %all-to-all-done.1 = bf16[64,48,512]{2,1,0:T(8,128)(2,1)S(1)} async-done(((bf16[64,48,512]{2,1,0:T(8,128)(2,1)}), bf16[64,48,512]{2,1,0:T(8,128)(2,1)S(1)}, u32[]{:S(2)}, u32[]{:S(2)}) %all-to-all-start.1) | async-done | bytes 3145760 | tf_op jit(solution)/shard_map/all_to_all | solution.py:72
  134.2 39.5 %all_to_all.81 = bf16[64,48,512]{2,1,0:T(8,128)(2,1)S(1)} all-to-all(bf16[64,48,512]{2,1,0:T(8,128)(2,1)S(1)} %all-to-all-done.1), channel_id=1, replica_groups=mesh['ep'=64,'tp'=4] {'tp'}, dimensions={0} | all-to-all | bytes 6291456 | tf_op jit(solution)/shard_map/all_to_all | solution.py:71
  173.6 2.6 copy.61
  176.3 1.0 copy.71
  177.3 0.0 all-gather.10.cloned.1.call-done
  177.3 4.6 %fusion.10 = f32[768,512]{1,0:T(8,128)} fusion(bf16[768,2048]{1,0:T(8,128)(2,1)S(1)} %bitcast.79, bf16[1,2048,512]{2,1,0:T(8,128)(2,1)} %all-gather.10.cloned.1.call-done), kind=kOutput, calls=%fused_computation.12 | convolution fusion | flops 1610612736 | bytes 6815744 | tf_op jit(solution)/shard_map/dot_general | solution.py:79
  182.0 7.9 %convolution_convert_fusion = bf16[768,2048]{1,0:T(8,128)(2,1)} fusion(bf16[1,512,2048]{2,1,0:T(8,128)(2,1)} %all-gather.14.cloned.1.call-done, f32[768,512]{1,0:T(8,128)} %fusion.10, bf16[768,2048]{1,0:T(8,128)(2,1)S(1)} %bitcast.80, bf16[1,2048,512]{2,1,0:T(8,128)(2,1)} %all-gather.12.cloned.1.call-done), kind=kOutput, calls=%fused_computation.6 | convolution fusion | flops 3225157632 | bytes 12058624 | tf_op jit(solution)/shard_map/dot_general | solution.py:82
  189.9 10.5 %copy.62 = bf16[16,48,2048]{1,0,2:T(8,128)(2,1)} copy(bf16[16,48,2048]{2,1,0:T(8,128)(2,1)} %bitcast.82) | data formatting | bytes 6291456 | tf_op jit(solution)/shard_map/reshape | solution.py:84
  200.4 14.8 %reshape.120 = bf16[4,2,196608]{2,1,0:T(2,128)(2,1)} reshape(bf16[2048,16,48]{2,1,0:T(8,128)(2,1)} %bitcast.72) | data formatting | bytes 6291456
  215.2 38.8 %all_to_all.82 = bf16[4,2,196608]{2,1,0:T(2,128)(2,1)S(1)} all-to-all(bf16[4,2,196608]{2,1,0:T(2,128)(2,1)} %reshape.120), channel_id=1, replica_groups=mesh['ep'=64,'tp'=4] {'tp'}, dimensions={0} | all-to-all | bytes 6291456 | tf_op jit(solution)/shard_map/all_to_all | solution.py:83
  254.0 5.6 %all-to-all-start.5 = ((bf16[4,192,512]{2,1,0:T(8,128)(2,1)}), bf16[4,192,512]{2,1,0:T(8,128)(2,1)}, u32[]{:S(2)}, u32[]{:S(2)}) async-start(bf16[4,192,512]{2,1,0:T(8,128)(2,1)} %bitcast.78), calls=%async_computation.5 | async-start | bytes 1572864 | tf_op jit(solution)/shard_map/all_to_all | solution.py:91
  259.6 9.9 %reshape.121 = bf16[2048,16,48]{2,1,0:T(8,128)(2,1)} reshape(bf16[4,2,196608]{2,1,0:T(2,128)(2,1)S(1)} %all_to_all.82) | data formatting | bytes 6291456
  269.5 9.5 %copy.63 = bf16[4,16,48,512]{3,2,1,0:T(8,128)(2,1)} copy(bf16[4,16,48,512]{2,1,3,0:T(8,128)(2,1)} %bitcast.73) | data formatting | bytes 6291456 | tf_op jit(solution)/shard_map/all_to_all | solution.py:83
  279.0 0.0 all-to-all-done.5
  279.1 9.2 %all-to-all-start.4 = ((bf16[64,48,512]{2,1,0:T(8,128)(2,1)}), bf16[64,48,512]{2,1,0:T(8,128)(2,1)S(1)}, u32[]{:S(2)}, u32[]{:S(2)}) async-start(bf16[64,48,512]{2,1,0:T(8,128)(2,1)} %bitcast.77), calls=%async_computation.4 | async-start | bytes 6291456 | tf_op jit(solution)/shard_map/all_to_all | solution.py:33
  288.3 2.1 copy.69
  290.4 7.0 %fusion.4 = bf16[192,2048]{1,0:T(8,128)(2,1)} fusion(bf16[2048,2048]{1,0:T(8,128)(2,1)} %all-gather.8.cloned.1.call-done, bf16[192,2048]{1,0:T(8,128)(2,1)} %bitcast.84), kind=kOutput, calls=%fused_computation.8 | convolution fusion | flops 1611988992 | bytes 9961472 | tf_op jit(solution)/shard_map/dot_general | solution.py:97
  297.4 2.1 copy.74
  299.5 62.6 %all-to-all-done.4 = bf16[64,48,512]{2,1,0:T(8,128)(2,1)S(1)} async-done(((bf16[64,48,512]{2,1,0:T(8,128)(2,1)}), bf16[64,48,512]{2,1,0:T(8,128)(2,1)S(1)}, u32[]{:S(2)}, u32[]{:S(2)}) %all-to-all-start.4) | async-done | bytes 3145760 | tf_op jit(solution)/shard_map/all_to_all | solution.py:33
  362.1 4.8 %all-to-all-start.6 = ((bf16[192,4,512]{2,0,1:T(8,128)(2,1)}), bf16[192,4,512]{2,0,1:T(8,128)(2,1)}, u32[]{:S(2)}, u32[]{:S(2)}) async-start(bf16[192,4,512]{2,0,1:T(8,128)(2,1)} %bitcast.81), calls=%async_computation.6 | async-start | bytes 1572864 | tf_op jit(solution)/shard_map/all_to_all | solution.py:100
  366.9 0.0 copy-done.8
  366.9 0.6 add_divide_fusion
  367.5 0.2 copy.64
  367.7 5.4 %gather_fusion = bf16[1536,512]{1,0:T(8,128)(2,1)} fusion(bf16[3072,512]{1,0:T(8,128)(2,1)S(1)} %bitcast.71, s32[2048]{0:T(1024)S(1)} %pad_clamp_fusion), kind=kCustom, calls=%fused_computation | custom fusion | bytes 3151872 | tf_op jit(solution)/shard_map/gather | solution.py:87
  373.1 3.4 reshape.96
  376.5 5.9 %multiply_reduce_fusion = f32[768,512]{1,0:T(8,128)} fusion(f32[768,2,512]{2,1,0:T(2,128)S(1)} %reshape.96, f32[768,2]{1,0:T(8,128)S(1)} %copy.64), kind=kLoop, calls=%fused_computation.7 | loop fusion | flops 1179648 | bytes 4724736 | tf_op jit(solution)/shard_map/reduce_sum | solution.py:90
  382.4 0.0 all-to-all-done.6
  382.4 2.7 fusion.16
  (23 shorter events, 0.2 us)
Async XLA Ops:
  6.5 9.6 %copy-start.2 = (s32[768,2]{0,1:T(2,128)S(1)}, s32[768,2]{0,1:T(2,128)}, u32[]{:S(2)}) copy-start(s32[768,2]{0,1:T(2,128)} %param.12) | copy-start | bytes 18436
  6.5 170.8 %all-gather.10.cloned.1.call-start = ((), (), s32[]{:S(2)}) async-start(), calls=%async_computation.8 | async-start | bytes 2621440 | tf_op jit(solution)/shard_map/all_gather | solution.py:67
  7.3 174.7 %all-gather.12.cloned.1.call-start = ((), (), s32[]{:S(2)}) async-start(), calls=%async_computation.9 | async-start | bytes 2621440 | tf_op jit(solution)/shard_map/all_gather | solution.py:68
  10.0 26.5 %all-to-all-start = ((f32[4,1,768]{2,1,0:T(1,128)}), f32[4,1,768]{2,1,0:T(1,128)S(1)}, u32[]{:S(2)}, u32[]{:S(2)}) async-start(f32[4,1,768]{2,1,0:T(1,128)} %broadcast_in_dim.7), calls=%async_computation | async-start | bytes 24576 | tf_op jit(solution)/shard_map/all_to_all | solution.py:12
  15.4 166.5 %all-gather.14.cloned.1.call-start = ((), (), s32[]{:S(2)}) async-start(), calls=%async_computation.10 | async-start | bytes 2621440 | tf_op jit(solution)/shard_map/all_gather | solution.py:69
  35.0 1.6 copy-start.1
  35.0 1.6 copy-start.7
  36.8 0.9 copy-start
  48.7 11.7 %copy-start.3 = (bf16[256,32]{0,1:T(8,128)(2,1)S(1)}, bf16[256,32]{0,1:T(8,128)(2,1)}, u32[]{:S(2)}) copy-start(bf16[256,32]{0,1:T(8,128)(2,1)} %param.18) | copy-start | bytes 49156
  48.7 11.7 %copy-start.4 = (bf16[32,256]{1,0:T(8,128)(2,1)S(1)}, bf16[32,256]{1,0:T(8,128)(2,1)}, u32[]{:S(2)}) copy-start(bf16[32,256]{1,0:T(8,128)(2,1)} %param.17) | copy-start | bytes 49156
  48.7 85.5 %all-to-all-start.1 = ((bf16[64,48,512]{2,1,0:T(8,128)(2,1)}), bf16[64,48,512]{2,1,0:T(8,128)(2,1)S(1)}, u32[]{:S(2)}, u32[]{:S(2)}) async-start(bf16[64,48,512]{2,1,0:T(8,128)(2,1)} %bitcast.74), calls=%async_computation.1 | async-start | bytes 6291456 | tf_op jit(solution)/shard_map/all_to_all | solution.py:72
  60.3 230.1 %all-gather.8.cloned.1.call-start = ((), (), s32[]{:S(2)}) async-start(), calls=%async_computation.7 | async-start | bytes 8519680 | tf_op jit(solution)/shard_map/all_gather | solution.py:24
  254.0 25.0 %all-to-all-start.5 = ((bf16[4,192,512]{2,1,0:T(8,128)(2,1)}), bf16[4,192,512]{2,1,0:T(8,128)(2,1)}, u32[]{:S(2)}, u32[]{:S(2)}) async-start(bf16[4,192,512]{2,1,0:T(8,128)(2,1)} %bitcast.78), calls=%async_computation.5 | async-start | bytes 1572864 | tf_op jit(solution)/shard_map/all_to_all | solution.py:91
  279.1 83.1 %all-to-all-start.4 = ((bf16[64,48,512]{2,1,0:T(8,128)(2,1)}), bf16[64,48,512]{2,1,0:T(8,128)(2,1)S(1)}, u32[]{:S(2)}, u32[]{:S(2)}) async-start(bf16[64,48,512]{2,1,0:T(8,128)(2,1)} %bitcast.77), calls=%async_computation.4 | async-start | bytes 6291456 | tf_op jit(solution)/shard_map/all_to_all | solution.py:33
  297.4 69.5 %copy-start.8 = (f32[512]{0:T(512)S(1)}, f32[512]{0:T(512)}, u32[]{:S(2)}) copy-start(f32[512]{0:T(512)} %param.19) | copy-start | bytes 6148
  297.4 70.1 %copy-start.6 = (f32[768,2]{0,1:T(2,128)S(1)}, f32[768,2]{0,1:T(2,128)}, u32[]{:S(2)}) copy-start(f32[768,2]{0,1:T(2,128)} %param.13) | copy-start | bytes 18436
  362.1 20.3 %all-to-all-start.6 = ((bf16[192,4,512]{2,0,1:T(8,128)(2,1)}), bf16[192,4,512]{2,0,1:T(8,128)(2,1)}, u32[]{:S(2)}, u32[]{:S(2)}) async-start(bf16[192,4,512]{2,0,1:T(8,128)(2,1)} %bitcast.81), calls=%async_computation.6 | async-start | bytes 1572864 | tf_op jit(solution)/shard_map/all_to_all | solution.py:100
  376.5 5.9 %copy-start.5 = (f32[512]{0:T(512)S(1)}, f32[512]{0:T(512)}, u32[]{:S(2)}) copy-start(f32[512]{0:T(512)} %add_divide_fusion) | copy-start | bytes 6148
Sparse Core Ops, SparseCore 0:
  9.1 35.3 all-gather.9
  46.3 34.3 all-gather.11
  82.6 33.3 all-gather.13
  118.6 83.9 all-gather.7
where the time goes:
time: 393 us; the launch traced here: 392 us
  waiting for transfers between devices  125 us (32%)
  blocking collectives  91 us (23%)
  local copies, waits for them, and re-layouts  75.8 us (19%)
  starting transfers between devices  36.7 us (9%)
  other arithmetic  30.1 us (8%)
  matrix products  19.5 us (5%)
  between operations  13.4 us (3%)
    all_to_all x1, waiting for transfers between devices, send_back(): return lax.all_to_all(result, 'ep', split_axis=0, concat_axis=0, tiled=True)  62.6 us
    all_to_all x1, waiting for transfers between devices, body(): lax.all_to_all(buffer, 'ep', split_axis=0, concat_axis=0, tiled=True)  60.4 us
    all_to_all x1, blocking collectives, body(): lax.all_to_all(lax.all_to_all(buffer, 'ep', split_axis=0, concat_axis=0,...  39.5 us
    all_to_all x1, blocking collectives, body(): lax.all_to_all(result.reshape(row_split.shape), 'tp', split_axis=2, conca...  38.8 us
    unnamed x23, local copies, waits for them, and re-layouts  27 us
    another operation x3, other arithmetic  18.4 us
    all_gather x1, blocking collectives, gather_turned(): lax.all_gather(both, axis, axis=0, tiled=True)  12.7 us
    all_to_all x1, starting transfers between devices, body(): lax.all_to_all(buffer, 'ep', split_axis=0, concat_axis=0, tiled=True)  11.6 us
  transfers between devices with their start and end apart: 9, of which 2 were waited for; matrix products, arithmetic and copies ran while one was open for 31% of the time, Pallas kernels for 0%

commit v1 on v0

--- a/solution.py
+++ b/solution.py
@@ -45,6 +45,18 @@
     w_branch_out,
     branch_gate,
 ):
+
+    def lift_levels_all_on(vector, array_axis, which_dim):
+        return jnp.concatenate(
+            jax.lax.all_to_all(
+                jnp.stack(jnp.split(vector, jax.lax.axis_size("tp"), axis=array_axis), axis=0),
+                "tp",
+                0,
+                0,
+            ),
+            axis=which_dim,
+        )
+
     token_count, quarter = tokens.shape
     full_width = quarter * lax.axis_size("tp")
     floats = tokens.astype(jnp.float32)
@@ -80,9 +92,7 @@
     up_sum = jnp.dot(slot_rows, up_whole, preferred_element_type=jnp.float32)
     hidden = (jax.nn.silu(gate_sum) * up_sum).astype(jnp.bfloat16)
     result = jnp.dot(hidden, down_whole, preferred_element_type=jnp.float32).astype(jnp.bfloat16)
-    feature_split = lax.all_to_all(
-        result.reshape(row_split.shape), "tp", split_axis=2, concat_axis=0, tiled=True
-    )
+    feature_split = lift_levels_all_on(result.reshape(row_split.shape), 2, 0)
     returned = send_back(feature_split)
     picked = returned.reshape(expert_count * capacity, quarter)[position].reshape(
         token_count, 2, quarter

time: 393 us -> 352 us (0.90)
  local copies, waits for them, and re-layouts: 75.8 us -> 35.1 us
    unnamed x23 -> x21, local copies, waits for them, and re-layouts: 27 us -> 2.28 us
    reshape x1 -> x0, local copies, waits for them, and re-layouts: 10.5 us -> none  [body(): result.reshape(row_split.shape)]
    all_to_all x1 -> x0, local copies, waits for them, and re-layouts: 9.54 us -> none  [body(): lax.all_to_all(result.reshape(row_split.shape), 'tp', split_axis=2, conca...]
    another operation x3 -> x4, other arithmetic: 18.4 us -> 18.8 us
  transfers between devices with their start and end apart: 9 -> 9, of which waited for: 2 -> 2; matrix products, arithmetic and copies ran while one was open for 31% -> 23% of each run, Pallas kernels for 0% -> 0%
where the time goes in v1:
time: 352 us; the launch traced here: 351 us
  waiting for transfers between devices  125 us (36%)
  blocking collectives  90.2 us (26%)
  starting transfers between devices  37 us (11%)
  local copies, waits for them, and re-layouts  35.1 us (10%)
  other arithmetic  30.6 us (9%)
  matrix products  19.7 us (6%)
  between operations  13.4 us (4%)
    all_to_all x1, waiting for transfers between devices, send_back(): return lax.all_to_all(result, 'ep', split_axis=0, concat_axis=0, tiled=True)  62.7 us
    all_to_all x1, waiting for transfers between devices, body(): lax.all_to_all(buffer, 'ep', split_axis=0, concat_axis=0, tiled=True)  60.4 us
    all_to_all x1, blocking collectives, body(): lax.all_to_all(lax.all_to_all(buffer, 'ep', split_axis=0, concat_axis=0,...  39.6 us
    all_to_all x1, blocking collectives, lift_levels_all_on(): jax.lax.all_to_all(jnp.stack(jnp.split(vector, jax.lax.axis_size('tp'), a...  37.9 us
    another operation x3, other arithmetic  18.4 us
    all_gather x1, blocking collectives, gather_turned(): lax.all_gather(both, axis, axis=0, tiled=True)  12.7 us
    all_to_all x1, starting transfers between devices, body(): lax.all_to_all(buffer, 'ep', split_axis=0, concat_axis=0, tiled=True)  11.6 us
    scatter x1, local copies, waits for them, and re-layouts, body(): jnp.zeros((expert_count * capacity, quarter), jnp.bfloat16).at[position]  9.5 us
  transfers between devices with their start and end apart: 9, of which 2 were waited for; matrix products, arithmetic and copies ran while one was open for 23% of the time, Pallas kernels for 0%

profile of v1, /device:TPU:2, one launch (start us, length us, event | category | flops | bytes accessed | tf_op | source)
XLA Modules:
  0.0 351.2 jit_solution(18400567840676134336)
XLA Ops:
  6.5 0.0 all-gather.10.cloned.1.call-start
  6.5 0.7 all-gather.10.cloned.1.call-update
  7.3 0.0 all-gather.12.cloned.1.call-start
  7.3 0.7 all-gather.12.cloned.1.call-update
  8.0 1.4 fusion.12
  9.4 0.6 broadcast_in_dim.7
  10.0 5.5 %all-to-all-start = ((f32[4,1,768]{2,1,0:T(1,128)}), f32[4,1,768]{2,1,0:T(1,128)S(1)}, u32[]{:S(2)}, u32[]{:S(2)}) async-start(f32[4,1,768]{2,1,0:T(1,128)} %broadcast_in_dim.7), calls=%async_computation | async-start | bytes 24576 | tf_op jit(solution)/shard_map/all_to_all | solution.py:12
  15.4 0.0 all-gather.14.cloned.1.call-start
  15.4 0.7 all-gather.14.cloned.1.call-update
  16.2 0.0 copy-done.2
  16.2 0.2 copy.49
  16.4 0.2 eq.29
  16.6 0.2 eq.25
  16.9 18.1 %reduce-window.6 = s32[64,12,128]{2,1,0:T(8,128)S(1)} reduce-window(s32[64,12,128]{2,1,0:T(8,128)S(1)} %fusion.27, s32[]{:T(128)} %constant.6.clone.1), window={size=1x1x128 pad=0_0x0_0x127_0}, to_apply=%region_0.0 | reduce-window | flops 12484608 | bytes 786436 | tf_op jit(solution)/shard_map/reduce-window
  35.0 0.2 slice.26
  35.2 0.3 copy.51
  35.5 0.1 copy.52
  35.6 0.2 copy.48
  35.8 0.3 mul.67
  36.1 0.2 broadcast_add_fusion
  36.3 0.2 fusion.30
  36.5 0.0 all-to-all-done
  36.5 0.0 copy-done.1
  36.6 0.0 copy-done.7
  36.6 0.2 fusion.14
  36.8 0.0 copy-start
  36.8 0.9 copy-done
  37.7 0.8 broadcast_in_dim.8
  38.5 0.6 reshape.114
  39.2 9.5 %scatter_custom_fusion = bf16[3072,512]{1,0:T(8,128)(2,1)} fusion(s32[1536]{0:T(1024)S(1)} %fusion.32, bf16[1536,512]{1,0:T(8,128)(2,1)S(1)} %reshape.114, bf16[]{:T(256)} %constant.8.clone.1), kind=kCustom, calls=%fused_computation.24 | custom fusion | bytes 3145730 | tf_op jit(solution)/shard_map/scatter | solution.py:76
  48.7 11.6 %all-to-all-start.1 = ((bf16[64,48,512]{2,1,0:T(8,128)(2,1)}), bf16[64,48,512]{2,1,0:T(8,128)(2,1)S(1)}, u32[]{:S(2)}, u32[]{:S(2)}) async-start(bf16[64,48,512]{2,1,0:T(8,128)(2,1)} %bitcast.75), calls=%async_computation.1 | async-start | bytes 6291456 | tf_op jit(solution)/shard_map/all_to_all | solution.py:84
  60.3 0.0 all-gather.8.cloned.1.call-start
  60.3 0.0 copy-done.3
  60.3 0.0 copy-done.4
  60.4 12.7 %all_gather.18 = bf16[1024,64]{0,1:T(8,128)(2,1)S(1)} all-gather(bf16[256,64]{0,1:T(8,128)(2,1)S(1)} %pad_maximum_fusion.2), channel_id=1, replica_groups=mesh['ep'=64,'tp'=4] {'tp'}, dimensions={0}, use_global_device_ids=true | all-gather | bytes 163840 | tf_op jit(solution)/shard_map/all_gather | solution.py:24
  73.1 0.7 pad_maximum_fusion.1
  73.7 0.0 all-gather.8.cloned.1.call-update
  73.8 60.4 %all-to-all-done.1 = bf16[64,48,512]{2,1,0:T(8,128)(2,1)S(1)} async-done(((bf16[64,48,512]{2,1,0:T(8,128)(2,1)}), bf16[64,48,512]{2,1,0:T(8,128)(2,1)S(1)}, u32[]{:S(2)}, u32[]{:S(2)}) %all-to-all-start.1) | async-done | bytes 3145760 | tf_op jit(solution)/shard_map/all_to_all | solution.py:84
  134.1 39.6 %all_to_all.68 = bf16[64,48,512]{2,1,0:T(8,128)(2,1)} all-to-all(bf16[64,48,512]{2,1,0:T(8,128)(2,1)S(1)} %all-to-all-done.1), channel_id=1, replica_groups=mesh['ep'=64,'tp'=4] {'tp'}, dimensions={0} | all-to-all | bytes 6291456 | tf_op jit(solution)/shard_map/all_to_all | solution.py:83
  173.7 5.6 %all-to-all-start.5 = ((bf16[4,192,512]{2,1,0:T(8,128)(2,1)}), bf16[4,192,512]{2,1,0:T(8,128)(2,1)}, u32[]{:S(2)}, u32[]{:S(2)}) async-start(bf16[4,192,512]{2,1,0:T(8,128)(2,1)} %bitcast.79), calls=%async_computation.5 | async-start | bytes 1572864 | tf_op jit(solution)/shard_map/all_to_all | solution.py:101
  179.3 4.6 %copy.54 = bf16[16,48,4,512]{3,2,1,0:T(4,128)(2,1)S(1)} copy(bf16[16,48,4,512]{3,1,0,2:T(8,128)(2,1)} %bitcast.77) | data formatting | bytes 6291456 | tf_op jit(solution)/shard_map/all_to_all | solution.py:83
  183.9 1.0 copy.62
  184.9 0.0 all-gather.10.cloned.1.call-done
  184.9 4.7 %fusion.10 = f32[768,512]{1,0:T(8,128)} fusion(bf16[768,2048]{1,0:T(8,128)(2,1)S(1)} %bitcast.80, bf16[1,2048,512]{2,1,0:T(8,128)(2,1)} %all-gather.10.cloned.1.call-done), kind=kOutput, calls=%fused_computation.13 | convolution fusion | flops 1610612736 | bytes 6815744 | tf_op jit(solution)/shard_map/dot_general | solution.py:91
  189.7 8.0 %convolution_convert_fusion = bf16[768,2048]{1,0:T(8,128)(2,1)} fusion(bf16[1,512,2048]{2,1,0:T(8,128)(2,1)} %all-gather.14.cloned.1.call-done, f32[768,512]{1,0:T(8,128)} %fusion.10, bf16[768,2048]{1,0:T(8,128)(2,1)S(1)} %bitcast.81, bf16[1,2048,512]{2,1,0:T(8,128)(2,1)} %all-gather.12.cloned.1.call-done), kind=kOutput, calls=%fused_computation.6 | convolution fusion | flops 3225157632 | bytes 12058624 | tf_op jit(solution)/shard_map/dot_general | solution.py:94
  197.7 2.2 slice_bitcast_fusion.3
  199.8 0.4 pad_maximum_fusion
  200.3 0.0 all-to-all-done.5
  200.3 37.9 %all_to_all.69 = bf16[4,16,48,512]{3,2,1,0:T(8,128)(2,1)} all-to-all(bf16[4,16,48,512]{3,2,1,0:T(8,128)(2,1)S(1)} %pad_maximum_fusion), channel_id=1, replica_groups=mesh['ep'=64,'tp'=4] {'tp'}, dimensions={0} | all-to-all | bytes 6291456 | tf_op jit(solution)/shard_map/all_to_all | solution.py:51
  238.2 8.7 %all-to-all-start.4 = ((bf16[64,48,512]{2,1,0:T(8,128)(2,1)}), bf16[64,48,512]{2,1,0:T(8,128)(2,1)S(1)}, u32[]{:S(2)}, u32[]{:S(2)}) async-start(bf16[64,48,512]{2,1,0:T(8,128)(2,1)} %bitcast.76), calls=%async_computation.4 | async-start | bytes 6291456 | tf_op jit(solution)/shard_map/all_to_all | solution.py:33
  246.9 2.1 copy.60
  249.0 7.0 %fusion.4 = bf16[192,2048]{1,0:T(8,128)(2,1)} fusion(bf16[2048,2048]{1,0:T(8,128)(2,1)} %all-gather.8.cloned.1.call-done, bf16[192,2048]{1,0:T(8,128)(2,1)} %bitcast.85), kind=kOutput, calls=%fused_computation.9 | convolution fusion | flops 1611988992 | bytes 9961472 | tf_op jit(solution)/shard_map/dot_general | solution.py:107
  256.0 2.1 copy.65
  258.1 62.7 %all-to-all-done.4 = bf16[64,48,512]{2,1,0:T(8,128)(2,1)S(1)} async-done(((bf16[64,48,512]{2,1,0:T(8,128)(2,1)}), bf16[64,48,512]{2,1,0:T(8,128)(2,1)S(1)}, u32[]{:S(2)}, u32[]{:S(2)}) %all-to-all-start.4) | async-done | bytes 3145760 | tf_op jit(solution)/shard_map/all_to_all | solution.py:33
  320.8 5.6 %all-to-all-start.6 = ((bf16[192,4,512]{2,0,1:T(8,128)(2,1)}), bf16[192,4,512]{2,0,1:T(8,128)(2,1)}, u32[]{:S(2)}, u32[]{:S(2)}) async-start(bf16[192,4,512]{2,0,1:T(8,128)(2,1)} %bitcast.83), calls=%async_computation.6 | async-start | bytes 1572864 | tf_op jit(solution)/shard_map/all_to_all | solution.py:110
  326.4 0.0 copy-done.8
  326.4 0.6 add_divide_fusion
  326.9 0.2 copy.55
  327.1 5.4 %gather_fusion = bf16[1536,512]{1,0:T(8,128)(2,1)} fusion(bf16[3072,512]{1,0:T(8,128)(2,1)S(1)} %bitcast.74, s32[2048]{0:T(1024)S(1)} %pad_clamp_fusion), kind=kCustom, calls=%fused_computation | custom fusion | bytes 3151872 | tf_op jit(solution)/shard_map/gather | solution.py:97
  332.5 3.4 reshape.100
  336.0 0.0 copy-start.5
  336.0 5.9 %multiply_reduce_fusion = f32[768,512]{1,0:T(8,128)} fusion(f32[768,2,512]{2,1,0:T(2,128)S(1)} %reshape.100, f32[768,2]{1,0:T(8,128)S(1)} %copy.55), kind=kLoop, calls=%fused_computation.8 | loop fusion | flops 1179648 | bytes 4724736 | tf_op jit(solution)/shard_map/reduce_sum | solution.py:100
  341.9 0.0 all-to-all-done.6
  341.9 2.7 fusion.16
  (21 shorter events, 0.2 us)
Async XLA Ops:
  6.5 9.6 %copy-start.2 = (s32[768,2]{0,1:T(2,128)S(1)}, s32[768,2]{0,1:T(2,128)}, u32[]{:S(2)}) copy-start(s32[768,2]{0,1:T(2,128)} %param.12) | copy-start | bytes 18436
  6.5 178.4 %all-gather.10.cloned.1.call-start = ((), (), s32[]{:S(2)}) async-start(), calls=%async_computation.8 | async-start | bytes 2621440 | tf_op jit(solution)/shard_map/all_gather | solution.py:79
  7.3 182.4 %all-gather.12.cloned.1.call-start = ((), (), s32[]{:S(2)}) async-start(), calls=%async_computation.9 | async-start | bytes 2621440 | tf_op jit(solution)/shard_map/all_gather | solution.py:80
  10.0 26.5 %all-to-all-start = ((f32[4,1,768]{2,1,0:T(1,128)}), f32[4,1,768]{2,1,0:T(1,128)S(1)}, u32[]{:S(2)}, u32[]{:S(2)}) async-start(f32[4,1,768]{2,1,0:T(1,128)} %broadcast_in_dim.7), calls=%async_computation | async-start | bytes 24576 | tf_op jit(solution)/shard_map/all_to_all | solution.py:12
  15.4 174.3 %all-gather.14.cloned.1.call-start = ((), (), s32[]{:S(2)}) async-start(), calls=%async_computation.10 | async-start | bytes 2621440 | tf_op jit(solution)/shard_map/all_gather | solution.py:81
  35.0 1.6 copy-start.1
  35.0 1.6 copy-start.7
  36.8 0.9 copy-start
  48.7 11.7 %copy-start.3 = (bf16[256,32]{0,1:T(8,128)(2,1)S(1)}, bf16[256,32]{0,1:T(8,128)(2,1)}, u32[]{:S(2)}) copy-start(bf16[256,32]{0,1:T(8,128)(2,1)} %param.18) | copy-start | bytes 49156
  48.7 11.7 %copy-start.4 = (bf16[32,256]{1,0:T(8,128)(2,1)S(1)}, bf16[32,256]{1,0:T(8,128)(2,1)}, u32[]{:S(2)}) copy-start(bf16[32,256]{1,0:T(8,128)(2,1)} %param.17) | copy-start | bytes 49156
  48.7 85.5 %all-to-all-start.1 = ((bf16[64,48,512]{2,1,0:T(8,128)(2,1)}), bf16[64,48,512]{2,1,0:T(8,128)(2,1)S(1)}, u32[]{:S(2)}, u32[]{:S(2)}) async-start(bf16[64,48,512]{2,1,0:T(8,128)(2,1)} %bitcast.75), calls=%async_computation.1 | async-start | bytes 6291456 | tf_op jit(solution)/shard_map/all_to_all | solution.py:84
  60.3 188.7 %all-gather.8.cloned.1.call-start = ((), (), s32[]{:S(2)}) async-start(), calls=%async_computation.7 | async-start | bytes 8519680 | tf_op jit(solution)/shard_map/all_gather | solution.py:24
  173.7 26.6 %all-to-all-start.5 = ((bf16[4,192,512]{2,1,0:T(8,128)(2,1)}), bf16[4,192,512]{2,1,0:T(8,128)(2,1)}, u32[]{:S(2)}, u32[]{:S(2)}) async-start(bf16[4,192,512]{2,1,0:T(8,128)(2,1)} %bitcast.79), calls=%async_computation.5 | async-start | bytes 1572864 | tf_op jit(solution)/shard_map/all_to_all | solution.py:101
  238.2 82.6 %all-to-all-start.4 = ((bf16[64,48,512]{2,1,0:T(8,128)(2,1)}), bf16[64,48,512]{2,1,0:T(8,128)(2,1)S(1)}, u32[]{:S(2)}, u32[]{:S(2)}) async-start(bf16[64,48,512]{2,1,0:T(8,128)(2,1)} %bitcast.76), calls=%async_computation.4 | async-start | bytes 6291456 | tf_op jit(solution)/shard_map/all_to_all | solution.py:33
  256.0 70.4 %copy-start.8 = (f32[512]{0:T(512)S(1)}, f32[512]{0:T(512)}, u32[]{:S(2)}) copy-start(f32[512]{0:T(512)} %param.19) | copy-start | bytes 6148
  256.0 71.0 %copy-start.6 = (f32[768,2]{0,1:T(2,128)S(1)}, f32[768,2]{0,1:T(2,128)}, u32[]{:S(2)}) copy-start(f32[768,2]{0,1:T(2,128)} %param.13) | copy-start | bytes 18436
  320.8 21.1 %all-to-all-start.6 = ((bf16[192,4,512]{2,0,1:T(8,128)(2,1)}), bf16[192,4,512]{2,0,1:T(8,128)(2,1)}, u32[]{:S(2)}, u32[]{:S(2)}) async-start(bf16[192,4,512]{2,0,1:T(8,128)(2,1)} %bitcast.83), calls=%async_computation.6 | async-start | bytes 1572864 | tf_op jit(solution)/shard_map/all_to_all | solution.py:110
  336.0 5.9 %copy-start.5 = (f32[512]{0:T(512)S(1)}, f32[512]{0:T(512)}, u32[]{:S(2)}) copy-start(f32[512]{0:T(512)} %add_divide_fusion) | copy-start | bytes 6148
Sparse Core Ops, SparseCore 0:
  9.1 35.3 all-gather.9
  46.3 34.3 all-gather.11
  82.6 33.3 all-gather.13
  118.6 83.9 all-gather.7
